TPU v7x, 32 devices: a whole 2x2x4 slice. The times are simulated.
32 devices in a mesh: sp: 4 (over z), fs: 4 (over y, x), tp: 2 (over core).
Axes of the slice: x: 2, y: 2, z: 4, core: 2. Of those that a mesh axis runs over, the one named last changes fastest.
Arguments:
- tokens: bfloat16 [4, 1024, 2048], P('fs', 'sp', 'tp'), may hold values from -6 to 6
- norm_gain: float32 [2048], replicated, may hold values from 0.1 to 1.9
- ret_query: bfloat16 [2048, 1024], P('sp', 'tp'), may hold values from -0.125 to 0.125
- ret_key: bfloat16 [2048, 1024], P('sp', 'tp'), may hold values from -0.125 to 0.125
- ret_value: bfloat16 [2048, 1024], P('sp', 'tp'), may hold values from -0.125 to 0.125
- att_query: bfloat16 [2048, 1024], P('sp', 'tp'), may hold values from -0.125 to 0.125
- att_key: bfloat16 [2048, 256], P('sp', 'tp'), may hold values from -0.125 to 0.125
- att_value: bfloat16 [2048, 256], P('sp', 'tp'), may hold values from -0.125 to 0.125
- log_decay: float32 [4, 4, 1024], P('fs', 'tp', 'sp'), may hold values from -1 to 0
- start_state: float32 [4, 4, 256, 256], P('fs', 'tp'), may hold values from -12 to 12
- ret_gain: float32 [1024], P('tp'), may hold values from 0.1 to 1.9
- sink_logits: float32 [16], P('tp'), may hold values from 1 to 5
- ret_out: bfloat16 [1024, 2048], P('tp', 'fs'), may hold values from -0.1875 to 0.1875
- att_out: bfloat16 [1024, 2048], P('tp', 'fs'), may hold values from -1.5 to 1.5
Outputs:
- mixed: bfloat16 [4, 1024, 2048], P('fs', 'sp', 'tp')
All inputs are finite; a program needn't handle non-finite values.
Results may differ from a plain program's by a relative error of at most 0.015.
Values may be sent and summed in bfloat16 or wider, within the bound.
A program may use at most 128 MiB of HBM per device.

v0:
```python
import jax
import jax.numpy as jnp
from jax import lax
from jax.sharding import PartitionSpec as P

DK = 256
DV = 256
HD = 64
WINDOW = 128
BLOCK = 128
epsilon = 1e-06
exact_result = lax.Precision.HIGHEST


def carried_in(array, axis, combine, identity):
    peers, mine = (lax.axis_size(axis), lax.axis_index(axis))
    everything = jax.tree.map(
        lambda part, kind: lax.all_gather(part.astype(kind), axis),
        array,
        (jnp.bfloat16, jnp.bfloat16),
    )
    start = jax.tree.map(
        lambda part, zero: jnp.broadcast_to(jnp.asarray(zero, part.dtype), part.shape),
        array,
        identity,
    )

    def hop(k, before):
        reached = k < mine
        new = combine(
            before, jax.tree.map(lambda part, own: part[k].astype(own.dtype), everything, array)
        )
        return jax.tree.map(lambda a, b: jnp.where(reached, a, b), new, before)

    return lax.fori_loop(0, peers, hop, start)


def passed_along(block, axis, distance):
    devices = range(lax.axis_size(axis))
    route = [(i - distance, i) for i in devices if i - distance in devices]
    return lax.ppermute(block, axis, route)


def rotate(values, positions):
    half_dim = values.shape[-1] // 2
    inverse = 1.0 / 10000.0 ** (jnp.arange(half_dim, dtype=jnp.float32) / half_dim)
    angles = positions.astype(jnp.float32)[:, None] * inverse[None, :]
    cosine = jnp.cos(angles)[:, None, :]
    sine_table = jnp.sin(angles)[:, None, :]
    front_half = values[..., :half_dim]
    back_half = values[..., half_dim:]
    return jnp.concatenate(
        [
            front_half * cosine - back_half * sine_table,
            front_half * sine_table + back_half * cosine,
        ],
        axis=-1,
    )


def block_step(memory_state, inputs):
    queries, key_matrix_rows, value_matrix_rows, log_rates = inputs
    length_here = log_rates.shape[-1]
    causal = jnp.arange(length_here)[:, None] >= jnp.arange(length_here)[None, :]
    running_totals = jnp.cumsum(log_rates, axis=-1)
    relative = running_totals[:, :, None] - running_totals[:, None, :]
    weight = jnp.where(causal[None], jnp.exp(jnp.where(causal[None], relative, 0.0)), 0.0)
    score_matrix = (
        jnp.einsum("hqd,hkd->hqk", queries, key_matrix_rows, precision=exact_result) * weight
    )
    carried_state = jnp.einsum(
        "hqd,hdv->hqv",
        queries * jnp.exp(running_totals)[:, :, None],
        memory_state,
        precision=exact_result,
    )
    output_rows = (
        jnp.einsum("arf,afu->aru", score_matrix, value_matrix_rows, precision=exact_result)
        + carried_state
    )
    decay_factors = jnp.exp(running_totals[:, -1:] - running_totals)
    memory_state = memory_state * jnp.exp(running_totals[:, -1])[:, None, None] + jnp.einsum(
        "iwj,iwe->ije",
        key_matrix_rows * decay_factors[:, :, None],
        value_matrix_rows,
        precision=exact_result,
    )
    return (memory_state, output_rows)


def chain(earlier, later):
    return (earlier[0] * later[0], earlier[1] * later[0][:, None, None] + later[1])


def shards(
    tokens,
    norm_gain,
    ret_query,
    ret_key,
    ret_value,
    att_query,
    att_key,
    att_value,
    log_decay,
    start_state,
    ret_gain,
    sink_logits,
    ret_out,
    att_out,
):
    gathered = lax.all_gather(tokens[0], "tp", axis=1, tiled=True)
    row_count = gathered.shape[0]
    as_float = gathered.astype(jnp.float32)
    normed = (
        as_float
        * lax.rsqrt(jnp.mean(as_float * as_float, axis=-1, keepdims=True) + epsilon)
        * norm_gain
    ).astype(jnp.bfloat16)
    offset = lax.axis_index("sp") * row_count
    positions = offset + jnp.arange(row_count, dtype=jnp.int32)
    weights = (ret_query, ret_key, ret_value, att_query, att_key, att_value)
    pieces = (
        lax.all_gather(weights[0], "sp", axis=0, tiled=True),
        lax.all_gather(weights[1], "sp", axis=0, tiled=True),
        lax.all_gather(weights[2], "sp", axis=0, tiled=True),
        lax.all_gather(weights[3], "sp", axis=0, tiled=True),
        lax.all_gather(weights[4], "sp", axis=0, tiled=True),
        lax.all_gather(weights[5], "sp", axis=0, tiled=True),
    )
    projected = tuple(
        (jnp.dot(normed, piece, preferred_element_type=jnp.float32) for piece in pieces)
    )
    rounded = tuple((product_f.astype(jnp.bfloat16) for product_f in projected))
    projected = rounded[:3]
    head_count = projected[0].shape[1] // DK
    queries = rotate(projected[0].astype(jnp.float32).reshape(row_count, head_count, DK), positions)
    keys_rot = rotate(
        projected[1].astype(jnp.float32).reshape(row_count, head_count, DK), positions
    ) * DK ** (-0.5)
    values_f = projected[2].astype(jnp.float32).reshape(row_count, head_count, DV)
    log_rates = log_decay[0]
    count = row_count // BLOCK

    def blocked(array):
        return array.reshape(count, BLOCK, head_count, array.shape[-1]).transpose(0, 2, 1, 3)

    rates_blocked = log_rates.reshape(head_count, count, BLOCK).transpose(1, 0, 2)
    local_state, pieces = lax.scan(
        block_step,
        jnp.zeros((head_count, DK, DV), jnp.float32),
        (blocked(queries), blocked(keys_rot), blocked(values_f), rates_blocked),
    )
    local_out = pieces.transpose(0, 2, 1, 3).reshape(row_count, head_count, DV)
    running_totals = jnp.cumsum(log_rates, axis=-1)
    device_decay = jnp.exp(running_totals[:, -1])
    identity = (jnp.ones((head_count,), jnp.float32), jnp.zeros((head_count, DK, DV), jnp.float32))
    prior_decay, prior_state = carried_in((device_decay, local_state), "sp", chain, identity)
    incoming = prior_state + prior_decay[:, None, None] * start_state[0]
    retained = local_out + jnp.einsum(
        "thd,hdv->thv",
        queries * jnp.exp(running_totals).T[:, :, None],
        incoming,
        precision=exact_result,
    )
    centred = retained - jnp.mean(retained, axis=-1, keepdims=True)
    variance = jnp.mean(centred * centred, axis=-1, keepdims=True)
    ret_hidden = (
        (centred * lax.rsqrt(variance + epsilon)).reshape(row_count, head_count * DV) * ret_gain
    ).astype(jnp.bfloat16)
    att_queries, att_keys, att_values = rounded[3:]
    kv_heads = att_keys.shape[1] // HD
    groups = att_queries.shape[1] // HD // kv_heads
    earlier_keys, earlier_values = passed_along(
        (att_keys[row_count - WINDOW :], att_values[row_count - WINDOW :]), "sp", 1
    )
    extended_keys = jnp.concatenate([earlier_keys, att_keys], axis=0)
    extended_values = jnp.concatenate([earlier_values, att_values], axis=0)
    windows = row_count // WINDOW

    def banded(array):
        earlier = array[:row_count].reshape(windows, WINDOW, kv_heads, HD)
        current = array[WINDOW:].reshape(windows, WINDOW, kv_heads, HD)
        return jnp.concatenate([earlier, current], axis=1)

    key_band = banded(extended_keys)
    value_band = banded(extended_values)
    grouped_q = att_queries.reshape(windows, WINDOW, kv_heads, groups, HD)
    score_matrix = jnp.einsum(
        "nqhgd,nkhd->nhgqk", grouped_q, key_band, preferred_element_type=jnp.float32
    ) * HD ** (-0.5)
    query_index = WINDOW + jnp.arange(WINDOW)
    key_index = jnp.arange(2 * WINDOW)
    allowed = (key_index[None, :] <= query_index[:, None]) & (
        query_index[:, None] - key_index[None, :] < WINDOW
    )
    key_place = offset - WINDOW + jnp.arange(windows)[:, None] * WINDOW + key_index[None, :]
    visible = (allowed[None] & (key_place >= 0)[:, None, :])[:, None, None]
    expo = jnp.exp(jnp.where(visible, score_matrix, -1e30))
    summed = jnp.sum(expo, axis=-1, keepdims=True) + jnp.exp(sink_logits).reshape(
        1, kv_heads, groups, 1, 1
    )
    probs = (expo / summed).astype(jnp.bfloat16)
    attended = jnp.einsum(
        "nhgqk,nkhd->nqhgd", probs, value_band, preferred_element_type=jnp.float32
    )
    att_hidden = attended.astype(jnp.bfloat16).reshape(row_count, kv_heads * groups * HD)
    ret_width = ret_hidden.shape[1]
    joined = jnp.concatenate([ret_hidden, att_hidden], axis=1)[None]
    piece = lax.all_gather(joined, "fs", axis=0, tiled=True)
    product = jnp.einsum(
        "srh,hd->srd", piece[:, :, :ret_width], ret_out, preferred_element_type=jnp.float32
    )
    product = product + jnp.einsum(
        "srh,hd->srd", piece[:, :, ret_width:], att_out, preferred_element_type=jnp.float32
    )
    partial_rows = product.astype(jnp.bfloat16)
    regrouped = lax.all_to_all(partial_rows, "fs", split_axis=0, concat_axis=2, tiled=True)
    mixed = lax.psum_scatter(
        regrouped[0].astype(jnp.float32).astype(jnp.bfloat16), "tp", scatter_dimension=1, tiled=True
    )
    return mixed[None]


def solution(mesh):
    placed = (
        P("fs", "sp", "tp"),
        P(),
        P("sp", "tp"),
        P("sp", "tp"),
        P("sp", "tp"),
        P("sp", "tp"),
        P("sp", "tp"),
        P("sp", "tp"),
        P("fs", "tp", "sp"),
        P("fs", "tp", None, None),
        P("tp"),
        P("tp"),
        P("tp", "fs"),
        P("tp", "fs"),
    )
    return jax.shard_map(
        shards, mesh=mesh, in_specs=placed, out_specs=P("fs", "sp", "tp"), check_vma=False
    )
```

profile of v0, /device:TPU:0, one launch (start us, length us, event | category | flops | bytes accessed | tf_op | source)
XLA Modules:
  0.0 330.0 jit_solution(6295431087866726067)
XLA Ops:
  13.0 13.6 %all-reduce = bf16[8]{0:T(256)(128)(2,1)S(1)} all-reduce(bf16[8]{0:T(256)(128)(2,1)S(1)} %dynamic-update-slice), channel_id=3, replica_groups=mesh['sp'=4,'fs'=4,'tp'=2] {'sp'}, use_global_device_ids=true, to_apply=%add | all-reduce | flops 8 | bytes 32
  26.6 18.4 %all_gather.42 = bf16[2048,128]{1,0:T(8,128)(2,1)S(1)} all-gather(bf16[512,128]{1,0:T(8,128)(2,1)S(1)} %copy-done.12), channel_id=1, replica_groups=mesh['sp'=4,'fs'=4,'tp'=2] {'sp'}, dimensions={0}, use_global_device_ids=true | all-gather | bytes 655360 | tf_op jit(solution)/shard_map/all_gather | solution.py:127
  45.7 21.2 %all_gather.41 = bf16[2048,128]{1,0:T(8,128)(2,1)} all-gather(bf16[512,128]{1,0:T(8,128)(2,1)S(1)} %copy-done.13), channel_id=1, replica_groups=mesh['sp'=4,'fs'=4,'tp'=2] {'sp'}, dimensions={0}, use_global_device_ids=true | all-gather | bytes 655360 | tf_op jit(solution)/shard_map/all_gather | solution.py:128
  68.9 1.6 fusion.25
  70.5 1.7 convolution_convert_fusion.5
  72.9 2.6 collective-permute-start.1
  75.5 5.5 %all-gather.12.cloned.1.call-done = bf16[2048,512]{1,0:T(8,128)(2,1)} async-done(((bf16[512,512]{1,0:T(8,128)(2,1)}), bf16[2048,512]{1,0:T(8,128)(2,1)}) %all-gather.12.cloned.1.call-update) | async-done | bytes 2097168 | tf_op jit(solution)/shard_map/all_gather | solution.py:124
  80.9 2.3 fusion.31
  83.6 44.0 %all-gather.16.cloned.1.call-done = bf16[2048,512]{1,0:T(8,128)(2,1)} async-done(((bf16[512,512]{1,0:T(8,128)(2,1)}), bf16[2048,512]{1,0:T(8,128)(2,1)}) %all-gather.16.cloned.1.call-update) | async-done | bytes 2097168 | tf_op jit(solution)/shard_map/all_gather | solution.py:123
  127.6 2.7 fusion.33
  131.4 42.1 %all-gather.14.cloned.1.call-done = bf16[2048,512]{1,0:T(8,128)(2,1)} async-done(((bf16[512,512]{1,0:T(8,128)(2,1)}), bf16[2048,512]{1,0:T(8,128)(2,1)}) %all-gather.14.cloned.1.call-update) | async-done | bytes 2097168 | tf_op jit(solution)/shard_map/all_gather | solution.py:125
  173.6 2.7 fusion.32
  178.9 6.7 %while.29 = (s32[]{:T(128)}, f32[2,256,256]{2,1,0:T(8,128)S(1)}, f32[2,2,128,256]{3,2,1,0:T(8,128)}, f32[2,2,128]{2,1,0:T(2,128)S(1)}, f32[2,2,128,256]{3,2,0,1:...) while((s32[]{:T(128)}, f32[2,256,256]{2,1,0:T(8,128)S(1)}, ...), condition=%wide.region_3.4_spmd.clone, body=%wide.region_1.3_spmd.clone.sunk | while | flops 604880896 | bytes 4242084 | solution.py:148
  186.4 1.9 convolution_convert_fusion.6
  188.6 2.3 collective-permute-start
  194.9 24.5 %all-gather.18.cloned.1.call-done = bf16[2048,512]{1,0:T(8,128)(2,1)} async-done(((bf16[512,512]{1,0:T(8,128)(2,1)}), bf16[2048,512]{1,0:T(8,128)(2,1)}) %all-gather.18.cloned.1.call-update) | async-done | bytes 2097168 | tf_op jit(solution)/shard_map/all_gather | solution.py:126
  219.5 2.3 convolution_convert_fusion.1
  223.8 25.1 %all-gather.22.cloned.1.call-done = bf16[8,256,256]{2,1,0:T(8,128)(2,1)} async-done(((bf16[2,256,256]{2,1,0:T(8,128)(2,1)}), bf16[8,256,256]{2,1,0:T(8,128)(2,1)}) %all-gather.22.cloned.1.call-update) | async-done | bytes 1048592 | tf_op jit(solution)/shard_map/all_gather | solution.py:18
  248.9 4.6 %while.30 = (s32[]{:T(128)}, f32[2]{0:T(128)S(1)}, f32[2,256,256]{2,1,0:T(8,128)S(1)}, s32[]{:T(128)}, bf16[4,2]{1,0:T(4,128)(2,1)S(1)}, /*index=5*/bf16[4,2,256,256]{3,2,1,0:T(8,128)(2,1)}, s32[]{:T(128)}, s32[]{:T(128)}) while((s32[]{:T(128)}, f32[2]{0:T(128)S(1)}, f32[2,256,256]{2,1,0:T(8,128)S(1)}, s32[]{:T(128)}, ...), condition=%wide.region_7.8_spmd.clone, body=%wide.region_6.7_spmd.clone.sunk | while | flops 655372 | bytes 1310871 | solution.py:35
  255.9 34.5 %all-gather.24.cloned.1.call-done = bf16[1024,1024]{0,1:T(8,128)(2,1)} async-done(((bf16[256,1024]{0,1:T(8,128)(2,1)}), bf16[1024,1024]{0,1:T(8,128)(2,1)}) %all-gather.24.cloned.1.call-update) | async-done | bytes 2097168 | tf_op jit(solution)/shard_map/all_gather | solution.py:209
  290.4 2.9 copy.81
  295.1 16.7 %all_to_all.15 = bf16[4,256,512]{2,1,0:T(8,128)(2,1)S(1)} all-to-all(bf16[4,256,512]{2,1,0:T(8,128)(2,1)S(1)} %add_convert_fusion), channel_id=1, replica_groups=mesh['sp'=4,'fs'=4,'tp'=2] {'fs'}, dimensions={0} | all-to-all | bytes 2097152 | tf_op jit(solution)/shard_map/all_to_all | solution.py:217
  313.1 8.0 %reduce-scatter.2.cloned.1.call-done = bf16[256,1024]{0,1:T(8,128)(2,1)} async-done(((bf16[256,2048]{0,1:T(8,128)(2,1)}), bf16[256,1024]{0,1:T(8,128)(2,1)}) %reduce-scatter.2.cloned.1.call-update) | async-done | bytes 524304 | tf_op jit(solution)/shard_map/reduce_scatter | solution.py:218
  321.1 2.0 copy.83
  (162 shorter events, 36.5 us)
Async XLA Ops:
  6.5 286.8 %copy-start = (bf16[512,512]{1,0:T(8,128)(2,1)S(1)}, bf16[512,512]{1,0:T(8,128)(2,1)}, u32[]{:S(2)}) copy-start(bf16[512,512]{1,0:T(8,128)(2,1)} %param.30) | copy-start | bytes 1572868
  6.5 4.8 %copy-start.23 = (u32[32]{0:T(128)S(1)}, u32[32]{0:T(128)}, u32[]{:S(2)}) copy-start(u32[32]{0:T(128)} %constant.93) | copy-start | bytes 388
  6.5 20.1 %copy-start.12 = (bf16[512,128]{1,0:T(8,128)(2,1)S(1)}, bf16[512,128]{1,0:T(8,128)(2,1)}, u32[]{:S(2)}) copy-start(bf16[512,128]{1,0:T(8,128)(2,1)} %param.24) | copy-start | bytes 393220
  6.5 38.6 %copy-start.22 = (f32[8]{0:T(128)S(1)}, f32[8]{0:T(128)}, u32[]{:S(2)}) copy-start(f32[8]{0:T(128)} %param.29) | copy-start | bytes 100
  6.5 39.2 %copy-start.13 = (bf16[512,128]{1,0:T(8,128)(2,1)S(1)}, bf16[512,128]{1,0:T(8,128)(2,1)}, u32[]{:S(2)}) copy-start(bf16[512,128]{1,0:T(8,128)(2,1)} %param.25) | copy-start | bytes 393220
  6.6 62.3 %all-gather.20.cloned.1.call-start = ((), (), s32[]{:S(2)}) async-start(), calls=%async_computation.7 | async-start | bytes 1572864 | tf_op jit(solution)/shard_map/all_gather | solution.py:111
  7.3 73.6 %all-gather.12.cloned.1.call-start = ((), (), s32[]{:S(2)}) async-start(), calls=%async_computation.2 | async-start | bytes 2621440 | tf_op jit(solution)/shard_map/all_gather | solution.py:124
  8.0 62.5 %copy-start.20 = (f32[2048]{0:T(1024)S(1)}, f32[2048]{0:T(1024)}, u32[]{:S(2)}) copy-start(f32[2048]{0:T(1024)} %param.19) | copy-start | bytes 24580
  8.1 119.6 %all-gather.16.cloned.1.call-start = ((), (), s32[]{:S(2)}) async-start(), calls=%async_computation.4 | async-start | bytes 2621440 | tf_op jit(solution)/shard_map/all_gather | solution.py:123
  8.8 164.8 %all-gather.14.cloned.1.call-start = ((), (), s32[]{:S(2)}) async-start(), calls=%async_computation.3 | async-start | bytes 2621440 | tf_op jit(solution)/shard_map/all_gather | solution.py:125
  9.4 210.1 %all-gather.18.cloned.1.call-start = ((), (), s32[]{:S(2)}) async-start(), calls=%async_computation.5 | async-start | bytes 2621440 | tf_op jit(solution)/shard_map/all_gather | solution.py:126
  10.0 238.9 %all-gather.22.cloned.1.call-start = ((), (), s32[]{:S(2)}) async-start(), calls=%async_computation.8 | async-start | bytes 1310720 | tf_op jit(solution)/shard_map/all_gather | solution.py:18
  68.9 12.1 %copy-start.5 = (bf16[1,256,2048]{2,1,0:T(8,128)(2,1)S(1)}, bf16[1,256,2048]{2,1,0:T(8,128)(2,1)}, u32[]{:S(2)}) copy-start(bf16[1,256,2048]{2,1,0:T(8,128)(2,1)} %all-gather.20.cloned.1.call-done) | copy-start | bytes 3145732
  70.5 103.1 %copy-start.18 = (f32[256]{0:T(256)}, f32[256]{0:T(256)S(1)}, u32[]{:S(2)}) copy-start(f32[256]{0:T(256)S(1)} %add_rsqrt_fusion.1) | copy-start | bytes 3076
  72.2 11.0 %copy-start.10 = (bf16[256,128]{1,0:T(8,128)(2,1)}, bf16[256,128]{1,0:T(8,128)(2,1)S(1)}, u32[]{:S(2)}) copy-start(bf16[256,128]{1,0:T(8,128)(2,1)S(1)} %convolution_convert_fusion.5) | copy-start | bytes 196612
  72.9 118.2 %collective-permute-start.1 = (bf16[128,128]{1,0:T(8,128)(2,1)}, bf16[128,128]{1,0:T(8,128)(2,1)}, u32[]{:S(2)}, u32[]{:S(2)}) collective-permute-start(bf16[128,128]{1,0:T(8,128)(2,1)} %slice.64), channel_id=1, source_target_pairs={{0,8},{8,16},{16,24},{1,9},{9,17},{17,25},{2,10},{10,18},{18,26},{... | collective-permute-start | bytes 98312 | tf_op jit(solution)/shard_map/ppermute | solution.py:41
  178.8 7.6 %copy-start.19 = (f32[256]{0:T(256)S(1)}, f32[256]{0:T(256)}, u32[]{:S(2)}) copy-start(f32[256]{0:T(256)} %copy-done.18) | copy-start | bytes 3076
  178.8 7.6 %copy-start.21 = (f32[2048]{0:T(1024)S(1)}, f32[2048]{0:T(1024)}, u32[]{:S(2)}) copy-start(f32[2048]{0:T(1024)} %param.19) | copy-start | bytes 24580
  186.4 104.1 %all-gather.24.cloned.1.call-start = ((), (), s32[]{:S(2)}) async-start(), calls=%async_computation.9 | async-start | bytes 2621440 | tf_op jit(solution)/shard_map/all_gather | solution.py:209
  188.3 31.2 %copy-start.6 = (bf16[1,256,2048]{2,1,0:T(8,128)(2,1)S(1)}, bf16[1,256,2048]{2,1,0:T(8,128)(2,1)}, u32[]{:S(2)}) copy-start(bf16[1,256,2048]{2,1,0:T(8,128)(2,1)} %all-gather.20.cloned.1.call-done) | copy-start | bytes 3145732
  188.6 4.3 %collective-permute-start = (bf16[128,128]{1,0:T(8,128)(2,1)S(1)}, bf16[128,128]{1,0:T(8,128)(2,1)S(1)}, u32[]{:S(2)}, u32[]{:S(2)}) collective-permute-start(bf16[128,128]{1,0:T(8,128)(2,1)S(1)} %slice.63), channel_id=1, source_target_pairs={{0,8},{8,16},{16,24},{1,9},{9,17},{17,25},{2,10},{10,18},{18,26},{... | collective-permute-start | bytes 98312 | tf_op jit(solution)/shard_map/ppermute | solution.py:41
  194.9 27.2 %copy-start.14 = (pred[2,128,256]{1,2,0:T(8,128)(4,1)S(1)}, pred[2,128,256]{1,2,0:T(8,128)(4,1)}, u32[]{:S(2)}) copy-start(pred[2,128,256]{1,2,0:T(8,128)(4,1)} %broadcast_and_fusion) | copy-start | bytes 196612
  248.9 4.6 %copy-start.9 = (f32[1,2,256,256]{3,2,1,0:T(8,128)S(1)}, f32[1,2,256,256]{3,2,1,0:T(8,128)}, u32[]{:S(2)}) copy-start(f32[1,2,256,256]{3,2,1,0:T(8,128)} %param.27) | copy-start | bytes 1572868
  255.9 65.2 %reduce-scatter.2.cloned.1.call-start = ((), (), s32[]{:S(2)}) async-start(), calls=%async_computation.6 | async-start | bytes 1572864 | tf_op jit(solution)/shard_map/reduce_scatter | solution.py:218
  (10 other events, 21.6 us)
Sparse Core Ops, SparseCore 0:
  8.9 11.7 all-gather.19
  22.3 58.6 all-gather.11
  82.5 45.0 all-gather.15
  129.1 44.4 all-gather.13
  175.0 44.4 all-gather.17
  220.9 27.9 all-gather.21
  256.0 34.4 all-gather.23
  313.2 7.8 reduce-scatter.1
where the time goes:
time: 331 us; the launch traced here: 330 us
  waiting for transfers between devices  188 us (57%)
  blocking collectives  69.8 us (21%)
  matrix products  23 us (7%)
  local copies, waits for them, and re-layouts  16.4 us (5%)
  between operations  14.8 us (4%)
  other arithmetic  12.8 us (4%)
  starting transfers between devices  5.19 us (2%)
    all_gather x1, waiting for transfers between devices, shards(): lax.all_gather(weights[0], 'sp', axis=0, tiled=True)  44 us
    all_gather x1, waiting for transfers between devices, shards(): lax.all_gather(weights[2], 'sp', axis=0, tiled=True)  42.1 us
    all_gather x1, waiting for transfers between devices, shards(): piece = lax.all_gather(joined, 'fs', axis=0, tiled=True)  34.5 us
    all_gather x1, waiting for transfers between devices, carried_in(): lax.all_gather(part.astype(kind), axis)  25.1 us
    all_gather x1, waiting for transfers between devices, shards(): lax.all_gather(weights[3], 'sp', axis=0, tiled=True)  24.5 us
    all_gather x1, blocking collectives, shards(): lax.all_gather(weights[5], 'sp', axis=0, tiled=True)  21.2 us
    all_gather x1, blocking collectives, shards(): lax.all_gather(weights[4], 'sp', axis=0, tiled=True)  18.4 us
    all_to_all x1, blocking collectives, shards(): lax.all_to_all(partial_rows, 'fs', split_axis=0, concat_axis=2, tiled=True)  16.7 us
  transfers between devices with their start and end apart: 10, of which 8 were waited for; matrix products, arithmetic and copies ran while one was open for 11% of the time, Pallas kernels for 0%

commit v1 on v0

--- a/solution.py
+++ b/solution.py
@@ -119,11 +119,26 @@
     offset = lax.axis_index("sp") * row_count
     positions = offset + jnp.arange(row_count, dtype=jnp.int32)
     weights = (ret_query, ret_key, ret_value, att_query, att_key, att_value)
+
+    def slices_shape(target):
+        current_value = lax.axis_size("sp")
+        r_now, r2, odd = (current_value, lax.axis_index("sp"), target.shape[0])
+        tile_out = map(lambda to_i: (to_i, (to_i + 1) % r_now), range(r_now))
+        pages = list(tile_out)
+        far_arr = jnp.zeros((*target.shape[:0], r_now * odd, *target.shape[1:]), target.dtype)
+        high = target
+        for j in range(r_now):
+            block_now = (r2 - j) % r_now
+            far_arr = lax.dynamic_update_slice_in_dim(far_arr, high, block_now * odd, axis=0)
+            if j < r_now - 1:
+                high = lax.ppermute(high, "sp", pages)
+        return far_arr
+
     pieces = (
         lax.all_gather(weights[0], "sp", axis=0, tiled=True),
         lax.all_gather(weights[1], "sp", axis=0, tiled=True),
         lax.all_gather(weights[2], "sp", axis=0, tiled=True),
-        lax.all_gather(weights[3], "sp", axis=0, tiled=True),
+        slices_shape(weights[3]),
         lax.all_gather(weights[4], "sp", axis=0, tiled=True),
         lax.all_gather(weights[5], "sp", axis=0, tiled=True),
     )

time: 331 us -> 315 us (0.952)
  waiting for transfers between devices: 188 us -> 144 us
  local copies, waits for them, and re-layouts: 16.4 us -> 32 us
  starting transfers between devices: 5.19 us -> 11.8 us
  blocking collectives: 69.8 us -> 73.6 us
    all_gather x1 -> x0, waiting for transfers between devices: 24.5 us -> none  [shards(): lax.all_gather(weights[3], 'sp', axis=0, tiled=True)]
    all_gather x1, waiting for transfers between devices: 25.1 us -> 17.6 us  [carried_in(): lax.all_gather(part.astype(kind), axis)]
    dynamic_update_slice x0 -> x4, local copies, waits for them, and re-layouts: none -> 6.6 us  [slices_shape(): lax.dynamic_update_slice_in_dim(far_arr, high, block_now * odd, axis=0)]
    all_gather x1, waiting for transfers between devices: 5.46 us -> 0.01 us  [shards(): lax.all_gather(weights[1], 'sp', axis=0, tiled=True)]
    ppermute x0 -> x3, starting transfers between devices: none -> 4.12 us  [slices_shape(): high = lax.ppermute(high, 'sp', pages)]
  transfers between devices with their start and end apart: 10 -> 12, of which waited for: 8 -> 6; matrix products, arithmetic and copies ran while one was open for 11% -> 17% of each run, Pallas kernels for 0% -> 0%
where the time goes in v1:
time: 315 us; the launch traced here: 314 us
  waiting for transfers between devices  144 us (46%)
  blocking collectives  73.6 us (23%)
  local copies, waits for them, and re-layouts  32 us (10%)
  matrix products  24.4 us (8%)
  between operations  14.9 us (5%)
  other arithmetic  13.6 us (4%)
  starting transfers between devices  11.8 us (4%)
    all_gather x1, waiting for transfers between devices, shards(): lax.all_gather(weights[0], 'sp', axis=0, tiled=True)  40.8 us
    all_gather x1, waiting for transfers between devices, shards(): lax.all_gather(weights[2], 'sp', axis=0, tiled=True)  39.8 us
    all_gather x1, waiting for transfers between devices, shards(): piece = lax.all_gather(joined, 'fs', axis=0, tiled=True)  34.5 us
    all_gather x1, blocking collectives, shards(): lax.all_gather(weights[5], 'sp', axis=0, tiled=True)  22.2 us
    all_gather x1, blocking collectives, shards(): lax.all_gather(weights[4], 'sp', axis=0, tiled=True)  19.9 us
    all_gather x1, waiting for transfers between devices, carried_in(): lax.all_gather(part.astype(kind), axis)  17.6 us
    all_to_all x1, blocking collectives, shards(): lax.all_to_all(partial_rows, 'fs', split_axis=0, concat_axis=2, tiled=True)  16.7 us
    dot_general x6, matrix products, shards(): jnp.dot(normed, piece, preferred_element_type=jnp.float32)  15.1 us
  transfers between devices with their start and end apart: 12, of which 6 were waited for; matrix products, arithmetic and copies ran while one was open for 17% of the time, Pallas kernels for 0%

profile of v1, /device:TPU:0, one launch (start us, length us, event | category | flops | bytes accessed | tf_op | source)
XLA Modules:
  0.0 313.8 jit_solution(5642508713859263436)
XLA Ops:
  8.8 3.1 collective-permute-start.2
  14.9 14.8 %all-reduce = bf16[8]{0:T(256)(128)(2,1)S(1)} all-reduce(bf16[8]{0:T(256)(128)(2,1)S(1)} %dynamic-update-slice), channel_id=3, replica_groups=mesh['sp'=4,'fs'=4,'tp'=2] {'sp'}, use_global_device_ids=true, to_apply=%add | all-reduce | flops 8 | bytes 32
  30.4 19.9 %all_gather.39 = bf16[2048,128]{1,0:T(8,128)(2,1)S(1)} all-gather(bf16[512,128]{1,0:T(8,128)(2,1)S(1)} %copy-done.16), channel_id=1, replica_groups=mesh['sp'=4,'fs'=4,'tp'=2] {'sp'}, dimensions={0}, use_global_device_ids=true | all-gather | bytes 655360 | tf_op jit(solution)/shard_map/all_gather | solution.py:142
  51.0 22.2 %all_gather.38 = bf16[2048,128]{1,0:T(8,128)(2,1)} all-gather(bf16[512,128]{1,0:T(8,128)(2,1)S(1)} %copy-done.17), channel_id=1, replica_groups=mesh['sp'=4,'fs'=4,'tp'=2] {'sp'}, dimensions={0}, use_global_device_ids=true | all-gather | bytes 655360 | tf_op jit(solution)/shard_map/all_gather | solution.py:143
  78.3 1.9 constant_dynamic-update-slice_fusion.2
  86.6 4.1 %collective-permute-start.1 = (bf16[128,128]{1,0:T(8,128)(2,1)}, bf16[128,128]{1,0:T(8,128)(2,1)}, u32[]{:S(2)}, u32[]{:S(2)}) collective-permute-start(bf16[128,128]{1,0:T(8,128)(2,1)} %slice.64), channel_id=1, source_target_pairs={{0,8},{8,16},{16,24},{1,9},{9,17},{17,25},{2,10},{10,18},{18,26},{... | collective-permute-start | bytes 98312 | tf_op jit(solution)/shard_map/ppermute | solution.py:41
  91.5 3.0 collective-permute-start
  96.9 1.9 constant_dynamic-update-slice_fusion.1
  98.8 3.1 fusion.31
  103.3 40.8 %all-gather.15.cloned.1.call-done = bf16[2048,512]{1,0:T(8,128)(2,1)} async-done(((bf16[512,512]{1,0:T(8,128)(2,1)}), bf16[2048,512]{1,0:T(8,128)(2,1)}) %all-gather.15.cloned.1.call-update) | async-done | bytes 2097168 | tf_op jit(solution)/shard_map/all_gather | solution.py:138
  144.1 3.1 %fusion.33 = f32[256,512]{1,0:T(8,128)} fusion(bf16[2048,512]{1,0:T(8,128)(2,1)} %all-gather.15.cloned.1.call-done, bf16[1,256,2048]{2,1,0:T(8,128)(2,1)S(1)} %copy-done.5, f32[2048]{0:T(1024)S(1)} %copy-done.32, f32[256]{0:T(256)S(1)} %add_rsqrt_fusion.1), kind=kOutput, calls=%fused_computation.57 | convolution fusion | flops 539230208 | bytes 3679232 | tf_op jit(solution)/shard_map/dot_general | solution.py:146
  147.3 2.2 reshape.299
  149.5 39.8 %all-gather.13.cloned.1.call-done = bf16[2048,512]{1,0:T(8,128)(2,1)} async-done(((bf16[512,512]{1,0:T(8,128)(2,1)}), bf16[2048,512]{1,0:T(8,128)(2,1)}) %all-gather.13.cloned.1.call-update) | async-done | bytes 2097168 | tf_op jit(solution)/shard_map/all_gather | solution.py:140
  189.3 3.1 fusion.32
  196.1 8.9 %while.29 = (s32[]{:T(128)}, f32[2,256,256]{2,1,0:T(8,128)S(1)}, f32[2,2,128,256]{3,2,1,0:T(8,128)}, f32[2,2,128]{2,1,0:T(2,128)S(1)}, f32[2,2,128,256]{3,2,0,1:...) while((s32[]{:T(128)}, f32[2,256,256]{2,1,0:T(8,128)S(1)}, ...), condition=%wide.region_3.4_spmd.clone, body=%wide.region_1.3_spmd.clone.sunk | while | flops 604880896 | bytes 4242144 | solution.py:163
  208.0 1.9 constant_dynamic-update-slice_fusion
  209.9 2.4 convolution_convert_fusion.1
  215.1 17.6 %all-gather.19.cloned.1.call-done = bf16[8,256,256]{2,1,0:T(8,128)(2,1)} async-done(((bf16[2,256,256]{2,1,0:T(8,128)(2,1)}), bf16[8,256,256]{2,1,0:T(8,128)(2,1)}) %all-gather.19.cloned.1.call-update) | async-done | bytes 1048592 | tf_op jit(solution)/shard_map/all_gather | solution.py:18
  232.7 4.6 %while.30 = (s32[]{:T(128)}, f32[2]{0:T(128)S(1)}, f32[2,256,256]{2,1,0:T(8,128)S(1)}, s32[]{:T(128)}, bf16[4,2]{1,0:T(4,128)(2,1)S(1)}, /*index=5*/bf16[4,2,256,256]{3,2,1,0:T(8,128)(2,1)}, s32[]{:T(128)}, s32[]{:T(128)}) while((s32[]{:T(128)}, f32[2]{0:T(128)S(1)}, f32[2,256,256]{2,1,0:T(8,128)S(1)}, s32[]{:T(128)}, ...), condition=%wide.region_7.8_spmd.clone, body=%wide.region_6.7_spmd.clone.sunk | while | flops 655372 | bytes 1310871 | solution.py:35
  239.8 34.5 %all-gather.21.cloned.1.call-done = bf16[1024,1024]{0,1:T(8,128)(2,1)} async-done(((bf16[256,1024]{0,1:T(8,128)(2,1)}), bf16[1024,1024]{0,1:T(8,128)(2,1)}) %all-gather.21.cloned.1.call-update) | async-done | bytes 2097168 | tf_op jit(solution)/shard_map/all_gather | solution.py:224
  274.3 2.9 copy.81
  279.0 16.7 %all_to_all.15 = bf16[4,256,512]{2,1,0:T(8,128)(2,1)S(1)} all-to-all(bf16[4,256,512]{2,1,0:T(8,128)(2,1)S(1)} %add_convert_fusion), channel_id=1, replica_groups=mesh['sp'=4,'fs'=4,'tp'=2] {'fs'}, dimensions={0} | all-to-all | bytes 2097152 | tf_op jit(solution)/shard_map/all_to_all | solution.py:232
  297.0 8.0 %reduce-scatter.2.cloned.1.call-done = bf16[256,1024]{0,1:T(8,128)(2,1)} async-done(((bf16[256,2048]{0,1:T(8,128)(2,1)}), bf16[256,1024]{0,1:T(8,128)(2,1)}) %reduce-scatter.2.cloned.1.call-update) | async-done | bytes 524304 | tf_op jit(solution)/shard_map/reduce_scatter | solution.py:233
  304.9 2.0 copy.83
  (196 shorter events, 49.5 us)
Async XLA Ops:
  6.5 270.6 %copy-start = (bf16[512,512]{1,0:T(8,128)(2,1)S(1)}, bf16[512,512]{1,0:T(8,128)(2,1)}, u32[]{:S(2)}) copy-start(bf16[512,512]{1,0:T(8,128)(2,1)} %param.30) | copy-start | bytes 1572868
  6.5 23.8 %copy-start.16 = (bf16[512,128]{1,0:T(8,128)(2,1)S(1)}, bf16[512,128]{1,0:T(8,128)(2,1)}, u32[]{:S(2)}) copy-start(bf16[512,128]{1,0:T(8,128)(2,1)} %param.24) | copy-start | bytes 393220
  6.5 43.8 %copy-start.34 = (f32[8]{0:T(128)S(1)}, f32[8]{0:T(128)}, u32[]{:S(2)}) copy-start(f32[8]{0:T(128)} %param.29) | copy-start | bytes 100
  6.5 44.4 %copy-start.17 = (bf16[512,128]{1,0:T(8,128)(2,1)S(1)}, bf16[512,128]{1,0:T(8,128)(2,1)}, u32[]{:S(2)}) copy-start(bf16[512,128]{1,0:T(8,128)(2,1)} %param.25) | copy-start | bytes 393220
  6.6 73.7 %all-gather.17.cloned.1.call-start = ((), (), s32[]{:S(2)}) async-start(), calls=%async_computation.6 | async-start | bytes 1572864 | tf_op jit(solution)/shard_map/all_gather | solution.py:111
  7.3 91.5 %all-gather.11.cloned.1.call-start = ((), (), s32[]{:S(2)}) async-start(), calls=%async_computation.2 | async-start | bytes 2621440 | tf_op jit(solution)/shard_map/all_gather | solution.py:139
  8.0 136.1 %all-gather.15.cloned.1.call-start = ((), (), s32[]{:S(2)}) async-start(), calls=%async_computation.4 | async-start | bytes 2621440 | tf_op jit(solution)/shard_map/all_gather | solution.py:138
  8.8 65.9 %copy-start.10 = (bf16[512,512]{1,0:T(8,128)(2,1)S(1)}, bf16[512,512]{1,0:T(8,128)(2,1)}, u32[]{:S(2)}) copy-start(bf16[512,512]{1,0:T(8,128)(2,1)} %param.23) | copy-start | bytes 1572868
  8.8 180.5 %all-gather.13.cloned.1.call-start = ((), (), s32[]{:S(2)}) async-start(), calls=%async_computation.3 | async-start | bytes 2621440 | tf_op jit(solution)/shard_map/all_gather | solution.py:140
  8.8 69.4 %collective-permute-start.2 = (bf16[512,512]{1,0:T(8,128)(2,1)}, bf16[512,512]{1,0:T(8,128)(2,1)}, u32[]{:S(2)}, u32[]{:S(2)}) collective-permute-start(bf16[512,512]{1,0:T(8,128)(2,1)} %param.23), channel_id=1, source_target_pairs={{0,8},{8,16},{16,24},{24,0},{1,9},{9,17},{17,25},{25,1},{2,10},{10... | collective-permute-start | bytes 1572872 | tf_op jit(solution)/shard_map/ppermute | solution.py:134
  12.0 220.7 %all-gather.19.cloned.1.call-start = ((), (), s32[]{:S(2)}) async-start(), calls=%async_computation.7 | async-start | bytes 1310720 | tf_op jit(solution)/shard_map/all_gather | solution.py:18
  78.3 17.6 %collective-permute-start.3 = (bf16[512,512]{1,0:T(8,128)(2,1)}, bf16[512,512]{1,0:T(8,128)(2,1)}, u32[]{:S(2)}, u32[]{:S(2)}) collective-permute-start(bf16[512,512]{1,0:T(8,128)(2,1)} %collective-permute-done.2), channel_id=1, source_target_pairs={{0,8},{8,16},{16,24},{24,0},{1,9},{9,17},{17,25},{25,1},{2,10},{10... | collective-permute-start | bytes 1572872 | tf_op jit(solution)/shard_map/ppermute | solution.py:134
  81.8 107.5 %copy-start.28 = (f32[256]{0:T(256)}, f32[256]{0:T(256)S(1)}, u32[]{:S(2)}) copy-start(f32[256]{0:T(256)S(1)} %add_rsqrt_fusion.1) | copy-start | bytes 3076
  84.3 14.5 %copy-start.31 = (f32[2048]{0:T(1024)S(1)}, f32[2048]{0:T(1024)}, u32[]{:S(2)}) copy-start(f32[2048]{0:T(1024)} %param.19) | copy-start | bytes 24580
  85.9 12.9 %copy-start.12 = (bf16[256,128]{1,0:T(8,128)(2,1)}, bf16[256,128]{1,0:T(8,128)(2,1)S(1)}, u32[]{:S(2)}) copy-start(bf16[256,128]{1,0:T(8,128)(2,1)S(1)} %convolution_convert_fusion.6) | copy-start | bytes 196612
  86.6 119.4 %collective-permute-start.1 = (bf16[128,128]{1,0:T(8,128)(2,1)}, bf16[128,128]{1,0:T(8,128)(2,1)}, u32[]{:S(2)}, u32[]{:S(2)}) collective-permute-start(bf16[128,128]{1,0:T(8,128)(2,1)} %slice.64), channel_id=1, source_target_pairs={{0,8},{8,16},{16,24},{1,9},{9,17},{17,25},{2,10},{10,18},{18,26},{... | collective-permute-start | bytes 98312 | tf_op jit(solution)/shard_map/ppermute | solution.py:41
  91.5 115.5 %collective-permute-start = (bf16[128,128]{1,0:T(8,128)(2,1)}, bf16[128,128]{1,0:T(8,128)(2,1)}, u32[]{:S(2)}, u32[]{:S(2)}) collective-permute-start(bf16[128,128]{1,0:T(8,128)(2,1)} %slice.63), channel_id=1, source_target_pairs={{0,8},{8,16},{16,24},{1,9},{9,17},{17,25},{2,10},{10,18},{18,26},{... | collective-permute-start | bytes 98312 | tf_op jit(solution)/shard_map/ppermute | solution.py:41
  95.8 112.1 %collective-permute-start.4 = (bf16[512,512]{1,0:T(8,128)(2,1)}, bf16[512,512]{1,0:T(8,128)(2,1)}, u32[]{:S(2)}, u32[]{:S(2)}) collective-permute-start(bf16[512,512]{1,0:T(8,128)(2,1)} %collective-permute-done.3), channel_id=1, source_target_pairs={{0,8},{8,16},{16,24},{24,0},{1,9},{9,17},{17,25},{25,1},{2,10},{10... | collective-permute-start | bytes 1572872 | tf_op jit(solution)/shard_map/ppermute | solution.py:134
  98.8 45.3 %copy-start.32 = (f32[2048]{0:T(1024)S(1)}, f32[2048]{0:T(1024)}, u32[]{:S(2)}) copy-start(f32[2048]{0:T(1024)} %param.19) | copy-start | bytes 24580
  196.0 11.0 %copy-start.13 = (bf16[256,128]{1,0:T(8,128)(2,1)S(1)}, bf16[256,128]{1,0:T(8,128)(2,1)}, u32[]{:S(2)}) copy-start(bf16[256,128]{1,0:T(8,128)(2,1)} %copy-done.12) | copy-start | bytes 196612
  205.7 68.6 %all-gather.21.cloned.1.call-start = ((), (), s32[]{:S(2)}) async-start(), calls=%async_computation.8 | async-start | bytes 2621440 | tf_op jit(solution)/shard_map/all_gather | solution.py:224
  214.0 18.7 %copy-start.22 = (f32[2]{0:T(128)S(1)}, f32[2]{0:T(128)}, u32[]{:S(2)}) copy-start(f32[2]{0:T(128)} %custom-call.1) | copy-start | bytes 28
  214.0 18.7 %copy-start.25 = (bf16[4,2]{1,0:T(4,128)(2,1)S(1)}, bf16[4,2]{1,0:T(4,128)(2,1)}, u32[]{:S(2)}) copy-start(bf16[4,2]{1,0:T(4,128)(2,1)} %reshape.302) | copy-start | bytes 52
  239.7 65.2 %reduce-scatter.2.cloned.1.call-start = ((), (), s32[]{:S(2)}) async-start(), calls=%async_computation.5 | async-start | bytes 1572864 | tf_op jit(solution)/shard_map/reduce_scatter | solution.py:233
  (25 other events, 84.2 us)
Sparse Core Ops, SparseCore 0:
  8.9 11.7 all-gather.16
  22.3 65.8 all-gather.10
  89.8 54.3 all-gather.14
  145.6 43.6 all-gather.12
  205.9 26.7 all-gather.18
  239.8 34.4 all-gather.20
  297.1 7.8 reduce-scatter.1
